TPU v7x, 32 devices: a whole 2x2x4 slice. The times are simulated.
32 devices in a mesh: grp: 2 (over y), fs: 4 (over z), tp: 4 (over x, core).
Axes of the slice: x: 2, y: 2, z: 4, core: 2. Of those that a mesh axis runs over, the one named last changes fastest.
Arguments:
- tokens: bfloat16 [1536, 2048], P(('grp', 'tp')), parts along dimension 0, may hold values from -6 to 6
- routes: int32 [1536, 2], P(('grp', 'tp')), parts along dimension 0, may hold values from 0 to 3, all different within a row; in each aligned block of 192 rows (0 to 191, 192 to 383, ...) at most 128 rows name the same one
- route_weight: float32 [1536, 2], P(('grp', 'tp')), parts along dimension 0, may hold values from 0.2 to 1
- norm_gain: float32 [2048], P('fs'), may hold values from 0.1 to 1.9
- gate_train: float32 [4, 2048, 5632], P('tp', 'fs'), may hold values from -0.125 to 0.125
- up_train: float32 [4, 2048, 5632], P('tp', 'fs'), may hold values from -0.125 to 0.125
- down_train: float32 [4, 5632, 2048], P('tp', None, 'fs'), may hold values from -0.109375 to 0.109375
Outputs:
- gate_serve: bfloat16 [8, 2048, 5632], P(('grp', 'tp'), None, 'fs'), parts along dimension 0
- up_serve: bfloat16 [8, 2048, 5632], P(('grp', 'tp'), None, 'fs'), parts along dimension 0
- down_serve: bfloat16 [8, 5632, 2048], P(('grp', 'tp'), 'fs'), parts along dimension 0
- mixed: bfloat16 [1536, 2048], P(('grp', 'tp'), 'fs'), parts along dimension 0
There are 2 independent parts, one for each index of `grp`. A program takes and returns all parts, laid end to end along the dimension named above; an argument that names none is the same for every part. Nothing has to cross between parts.
Inputs may be any that keep to these rules, and one draw needn't show every extreme that they name: `routes`: each row names 2 different experts. In each aligned block of 192 rows no expert is named by more than 128 rows, a bound that some block reaches.
All inputs are finite; a program needn't handle non-finite values.
Results may differ from a plain program's by a relative error of at most 0.0087.
Values may be sent and summed in bfloat16 or wider, within the bound.
A program may use at most 128 MiB of HBM per device.

v0:
```python
import jax
import jax.numpy as jnp
from jax import lax
from jax.sharding import PartitionSpec as P

EXPERTS = 4
CAP = 128


def shards(tokens, routes, route_weight, norm_gain, gate_train, up_train, down_train):
    fs_count = lax.axis_size("fs")
    pieces = min(fs_count, 32)
    copies = fs_count // pieces
    gain_column = norm_gain[:, None]
    gate_low = (gate_train[0] * gain_column).astype(jnp.bfloat16)
    up_low = (up_train[0] * gain_column).astype(jnp.bfloat16)
    down_low = down_train[0].astype(jnp.bfloat16)
    gate_wide = jnp.tile(gate_low, (1, copies))
    up_wide = jnp.tile(up_low, (1, copies))
    down_wide = jnp.tile(down_low, (copies, 1))
    gate_new, up_new = (
        lax.all_to_all(gate_wide, "fs", split_axis=1, concat_axis=0, tiled=True),
        lax.all_to_all(up_wide, "fs", split_axis=1, concat_axis=0, tiled=True),
    )
    down_new = lax.all_to_all(down_wide, "fs", split_axis=0, concat_axis=1, tiled=True)
    tok_float = tokens.astype(jnp.float32)
    normed = (
        tok_float * lax.rsqrt(jnp.mean(tok_float * tok_float, axis=-1, keepdims=True) + 1e-06)
    ).astype(jnp.bfloat16)
    chosen = routes.reshape(-1)
    chosen_hot = (chosen[:, None] == jnp.arange(EXPERTS, dtype=jnp.int32)[None, :]).astype(
        jnp.int32
    )
    before = jnp.cumsum(chosen_hot, axis=0) - chosen_hot
    slot_rank = jnp.sum(before * chosen_hot, axis=1)
    slot_index = (chosen * CAP + slot_rank).reshape(routes.shape)
    slot_range = jnp.arange(EXPERTS * CAP, dtype=jnp.int32)
    select_rows = jnp.any(slot_range[:, None, None] == slot_index[None, :, :], axis=-1).astype(
        jnp.bfloat16
    )
    outgoing = jnp.dot(select_rows, normed, preferred_element_type=jnp.float32).astype(jnp.bfloat16)
    outgoing = outgoing.reshape(EXPERTS, CAP, normed.shape[1])
    arrived = lax.all_to_all(outgoing, "tp", split_axis=0, concat_axis=0, tiled=True).reshape(
        EXPERTS * CAP, normed.shape[1]
    )
    slot_count = EXPERTS * CAP // copies
    copy_index = lax.axis_index("fs") // pieces
    my_rows = lax.dynamic_slice_in_dim(arrived, copy_index * slot_count, slot_count, 0)
    gated = jnp.dot(my_rows, gate_new, preferred_element_type=jnp.float32)
    lifted = jnp.dot(my_rows, up_new, preferred_element_type=jnp.float32)
    hidden = (jax.nn.silu(gated) * lifted).astype(jnp.bfloat16)
    partial_out = jnp.dot(hidden, down_new, preferred_element_type=jnp.float32)
    placed = jnp.zeros((EXPERTS * CAP, partial_out.shape[1]), jnp.float32)
    placed = lax.dynamic_update_slice_in_dim(placed, partial_out, copy_index * slot_count, 0)
    expert_out = lax.psum_scatter(placed, "fs", scatter_dimension=1, tiled=True).astype(
        jnp.bfloat16
    )
    returned = lax.all_to_all(
        expert_out.reshape(EXPERTS, CAP, expert_out.shape[1]),
        "tp",
        split_axis=0,
        concat_axis=0,
        tiled=True,
    )
    returned = returned.reshape(EXPERTS * CAP, expert_out.shape[1]).astype(jnp.float32)
    blend_weight = jnp.sum(
        jnp.where(
            slot_range[None, None, :] == slot_index[:, :, None], route_weight[:, :, None], 0.0
        ),
        axis=1,
    )
    mixed = jnp.dot(
        blend_weight, returned, precision=lax.Precision.HIGHEST, preferred_element_type=jnp.float32
    )
    return (gate_new[None], up_new[None], down_new[None], mixed.astype(jnp.bfloat16))


def solution(mesh):
    in_specs = (
        P(("grp", "tp"), None),
        P(("grp", "tp"), None),
        P(("grp", "tp"), None),
        P("fs"),
        P("tp", "fs", None),
        P("tp", "fs", None),
        P("tp", None, "fs"),
    )
    out_specs = (
        P(("grp", "tp"), None, "fs"),
        P(("grp", "tp"), None, "fs"),
        P(("grp", "tp"), "fs", None),
        P(("grp", "tp"), "fs"),
    )
    return jax.shard_map(shards, mesh=mesh, in_specs=in_specs, out_specs=out_specs, check_vma=False)
```

profile of v0, /device:TPU:0, one launch (start us, length us, event | category | flops | bytes accessed | tf_op | source)
XLA Modules:
  0.0 587.4 jit_solution(4837379173826643466)
XLA Ops:
  7.2 0.8 copy.54
  8.0 0.1 eq.56
  8.3 1.2 reduce-window.6
  9.5 0.2 slice_reduce_fusion
  9.7 0.2 reduce-window.9
  10.0 0.1 reduce_sum.30
  10.2 0.7 multiply_add_fusion
  11.1 1.4 fusion.3
  12.4 3.3 convolution_convert_fusion
  15.7 4.2 all-to-all-start.3
  19.9 14.5 %squeeze.7 = f32[512,4,1408]{2,1,0:T(4,128)} reshape(f32[1,512,5632]{2,1,0:T(8,128)} %param.11) | data formatting | bytes 23068672 | tf_op jit(solution)/shard_map/squeeze | solution.py:15
  34.5 14.5 %squeeze.8 = f32[512,4,1408]{2,1,0:T(4,128)} reshape(f32[1,512,5632]{2,1,0:T(8,128)} %param.12) | data formatting | bytes 23068672 | tf_op jit(solution)/shard_map/squeeze | solution.py:16
  49.0 16.8 %fusion = (bf16[512,4,1408]{2,0,1:T(8,128)(2,1)}, bf16[512,4,1408]{2,0,1:T(8,128)(2,1)}) fusion(f32[512,4,1408]{2,1,0:T(4,128)} %squeeze.8, f32[512]{0:T(512)S(1)} %copy-done, f32[512,4,1408]{2,1,0:T(4,128)} %squeeze.7), kind=kLoop, calls=%fused_computation.1 | loop fusion | flops 11534336 | bytes 34605056 | tf_op jit(solution)/shard_map/convert_element_type | solution.py:16
  65.9 5.7 all-to-all-start
  71.6 7.5 %convert_element_type.44 = bf16[1,5632,512]{2,1,0:T(8,128)(2,1)} convert(f32[1,5632,512]{2,1,0:T(8,128)} %param.13) | non-fusion elementwise | flops 2883584 | bytes 17301504 | tf_op jit(solution)/shard_map/convert_element_type | solution.py:17
  79.1 120.5 %all-to-all-done = bf16[512,4,1408]{2,0,1:T(8,128)(2,1)} async-done(((bf16[512,4,1408]{2,0,1:T(8,128)(2,1)}), bf16[512,4,1408]{2,0,1:T(8,128)(2,1)}, u32[]{:S(2)}, u32[]{:S(2)}) %all-to-all-start) | async-done | bytes 5767200 | tf_op jit(solution)/shard_map/all_to_all | solution.py:22
  199.6 133.5 %all_to_all.58 = bf16[4,1408,512]{2,1,0:T(8,128)(2,1)} all-to-all(bf16[4,1408,512]{2,1,0:T(8,128)(2,1)} %bitcast.49), channel_id=1, replica_groups=mesh['grp'=2,'fs'=4,'tp'=4] {'fs'}, dimensions={0} | all-to-all | bytes 11534336 | tf_op jit(solution)/shard_map/all_to_all | solution.py:25
  333.2 5.2 all-to-all-start.1
  338.3 0.2 reduce-scatter.2.cloned.1.call-start
  338.6 8.3 %copy.53 = bf16[4,1408,512]{1,2,0:T(8,128)(2,1)} copy(bf16[4,1408,512]{2,1,0:T(8,128)(2,1)} %all_to_all.58) | data formatting | bytes 11534336 | tf_op jit(solution)/shard_map/all_to_all | solution.py:25
  346.9 7.6 %fusion.14 = f32[512,1408]{1,0:T(8,128)} fusion(bf16[512,2048]{1,0:T(8,128)(2,1)S(1)} %bitcast.50, bf16[2048,1408]{1,0:T(8,128)(2,1)} %bitcast.10), kind=kOutput, calls=%fused_computation.30 | convolution fusion | flops 2952790016 | bytes 10747904 | tf_op jit(solution)/shard_map/dot_general | solution.py:49
  354.5 110.3 %all-to-all-done.1 = bf16[512,4,1408]{2,0,1:T(8,128)(2,1)} async-done(((bf16[512,4,1408]{2,0,1:T(8,128)(2,1)}), bf16[512,4,1408]{2,0,1:T(8,128)(2,1)}, u32[]{:S(2)}, u32[]{:S(2)}) %all-to-all-start.1) | async-done | bytes 5767200 | tf_op jit(solution)/shard_map/all_to_all | solution.py:23
  464.8 13.9 %fusion.8 = f32[512,2048]{1,0:T(8,128)} fusion(bf16[1408,2048]{0,1:T(8,128)(2,1)} %bitcast.47, bf16[512,2048]{1,0:T(8,128)(2,1)S(1)} %bitcast.51, bf16[2048,1408]{1,0:T(8,128)(2,1)} %bitcast.11, f32[512,1408]{1,0:T(8,128)} %fusion.14), kind=kOutput, calls=%fused_computation.17 | convolution fusion | flops 5909905408 | bytes 20709376 | tf_op jit(solution)/shard_map/dot_general | solution.py:52
  478.7 75.2 %reduce-scatter.2.cloned.1.call-done = f32[512,512]{1,0:T(8,128)} async-done(((f32[512,2048]{1,0:T(8,128)}), f32[512,512]{1,0:T(8,128)}) %reduce-scatter.2.cloned.1.call-update) | async-done | bytes 1048592 | tf_op jit(solution)/shard_map/reduce_scatter | solution.py:55
  553.9 2.1 convert_element_type.52
  555.9 3.5 all-to-all-start.4
  559.4 0.2 select_reduce_fusion
  559.6 8.2 %copy.57 = bf16[1,1408,2048]{2,1,0:T(8,128)(2,1)} copy(bf16[1,1408,2048]{1,2,0:T(8,128)(2,1)} %bitcast.48) | data formatting | bytes 11534336
  567.9 0.3 all-to-all-done.4
  568.2 1.2 convolution_convert_fusion.1
  569.4 5.6 copy.68
  575.0 5.6 copy.69
  (13 shorter events, 0.5 us)
Async XLA Ops:
  15.7 50.1 %all-to-all-start.3 = ((bf16[4,128,2048]{2,1,0:T(8,128)(2,1)}), bf16[4,128,2048]{2,1,0:T(8,128)(2,1)S(1)}, u32[]{:S(2)}, u32[]{:S(2)}) async-start(bf16[4,128,2048]{2,1,0:T(8,128)(2,1)} %bitcast.8), calls=%async_computation.3 | async-start | bytes 4194304 | tf_op jit(solution)/shard_map/all_to_all | solution.py:43
  34.5 14.5 %copy-start = (f32[512]{0:T(512)S(1)}, f32[512]{0:T(512)}, u32[]{:S(2)}) copy-start(f32[512]{0:T(512)} %param.10) | copy-start | bytes 6148
  65.9 133.8 %all-to-all-start = ((bf16[512,4,1408]{2,0,1:T(8,128)(2,1)}), bf16[512,4,1408]{2,0,1:T(8,128)(2,1)}, u32[]{:S(2)}, u32[]{:S(2)}) async-start(bf16[512,4,1408]{2,0,1:T(8,128)(2,1)} %get-tuple-element.17), calls=%async_computation | async-start | bytes 11534336 | tf_op jit(solution)/shard_map/all_to_all | solution.py:22
  333.2 131.6 %all-to-all-start.1 = ((bf16[512,4,1408]{2,0,1:T(8,128)(2,1)}), bf16[512,4,1408]{2,0,1:T(8,128)(2,1)}, u32[]{:S(2)}, u32[]{:S(2)}) async-start(bf16[512,4,1408]{2,0,1:T(8,128)(2,1)} %get-tuple-element.16), calls=%async_computation.1 | async-start | bytes 11534336 | tf_op jit(solution)/shard_map/all_to_all | solution.py:23
  338.3 215.5 %reduce-scatter.2.cloned.1.call-start = ((), (), s32[]{:S(2)}) async-start(), calls=%async_computation.6 | async-start | bytes 5242880 | tf_op jit(solution)/shard_map/reduce_scatter | solution.py:55
  478.7 80.8 %copy-start.1 = (f32[192,2]{0,1:T(2,128)S(1)}, f32[192,2]{0,1:T(2,128)}, u32[]{:S(2)}) copy-start(f32[192,2]{0,1:T(2,128)} %param.9) | copy-start | bytes 4612
  555.9 12.3 %all-to-all-start.4 = ((bf16[4,128,512]{2,1,0:T(8,128)(2,1)}), bf16[4,128,512]{2,1,0:T(8,128)(2,1)S(1)}, u32[]{:S(2)}, u32[]{:S(2)}) async-start(bf16[4,128,512]{2,1,0:T(8,128)(2,1)} %bitcast.13), calls=%async_computation.5 | async-start | bytes 1048576 | tf_op jit(solution)/shard_map/all_to_all | solution.py:58
Sparse Core Ops, SparseCore 0:
  478.8 74.9 reduce-scatter.1
where the time goes:
time: 589 us; the launch traced here: 587 us
  waiting for transfers between devices  306 us (52%)
  blocking collectives  134 us (23%)
  local copies, waits for them, and re-layouts  58.3 us (10%)
  other arithmetic  30.4 us (5%)
  matrix products  25.9 us (4%)
  starting transfers between devices  18.8 us (3%)
  between operations  14.1 us (2%)
    all_to_all x1, blocking collectives, shards(): lax.all_to_all(down_wide, 'fs', split_axis=0, concat_axis=1, tiled=True)  134 us
    all_to_all x1, waiting for transfers between devices, shards(): lax.all_to_all(gate_wide, 'fs', split_axis=1, concat_axis=0, tiled=True)  120 us
    all_to_all x1, waiting for transfers between devices, shards(): lax.all_to_all(up_wide, 'fs', split_axis=1, concat_axis=0, tiled=True)  110 us
    reduce_scatter x1, waiting for transfers between devices, shards(): lax.psum_scatter(placed, 'fs', scatter_dimension=1, tiled=True)  75.2 us
    unnamed x8, local copies, waits for them, and re-layouts  20.2 us
    convert_element_type x1, other arithmetic, shards(): up_low = (up_train[0] * gain_column).astype(jnp.bfloat16)  16.8 us
    squeeze x1, local copies, waits for them, and re-layouts, shards(): gate_low = (gate_train[0] * gain_column).astype(jnp.bfloat16)  14.5 us
    squeeze x1, local copies, waits for them, and re-layouts, shards(): up_low = (up_train[0] * gain_column).astype(jnp.bfloat16)  14.5 us
  transfers between devices with their start and end apart: 5, of which 4 were waited for; matrix products, arithmetic and copies ran while one was open for 13% of the time, Pallas kernels for 0%

commit v1 on v0

--- a/solution.py
+++ b/solution.py
@@ -22,7 +22,10 @@
         lax.all_to_all(gate_wide, "fs", split_axis=1, concat_axis=0, tiled=True),
         lax.all_to_all(up_wide, "fs", split_axis=1, concat_axis=0, tiled=True),
     )
-    down_new = lax.all_to_all(down_wide, "fs", split_axis=0, concat_axis=1, tiled=True)
+    down_new = jnp.concatenate(
+        lax.all_to_all(jnp.stack(jnp.split(down_wide, lax.axis_size("fs"), axis=0)), "fs", 0, 0),
+        axis=1,
+    )
     tok_float = tokens.astype(jnp.float32)
     normed = (
         tok_float * lax.rsqrt(jnp.mean(tok_float * tok_float, axis=-1, keepdims=True) + 1e-06)

time: 589 us -> 590 us (level)
    unnamed x8 -> x9, local copies, waits for them, and re-layouts: 20.2 us -> 29.8 us
    all_to_all x1 -> x0, local copies, waits for them, and re-layouts: 8.34 us -> none  [shards(): lax.all_to_all(down_wide, 'fs', split_axis=0, concat_axis=1, tiled=True)]
    convert_element_type x1 -> x0, other arithmetic: 7.55 us -> none  [shards(): down_low = down_train[0].astype(jnp.bfloat16)]
where the time goes in v1:
time: 590 us; the launch traced here: 588 us
  waiting for transfers between devices  306 us (52%)
  blocking collectives  135 us (23%)
  local copies, waits for them, and re-layouts  62.7 us (11%)
  other arithmetic  26.1 us (4%)
  matrix products  25.9 us (4%)
  starting transfers between devices  18.2 us (3%)
  between operations  14.1 us (2%)
    all_to_all x1, blocking collectives, shards(): lax.all_to_all(gate_wide, 'fs', split_axis=1, concat_axis=0, tiled=True)  135 us
    all_to_all x1, waiting for transfers between devices, shards(): lax.all_to_all(jnp.stack(jnp.split(down_wide, lax.axis_size('fs'), axis=0...  119 us
    all_to_all x1, waiting for transfers between devices, shards(): lax.all_to_all(up_wide, 'fs', split_axis=1, concat_axis=0, tiled=True)  111 us
    reduce_scatter x1, waiting for transfers between devices, shards(): lax.psum_scatter(placed, 'fs', scatter_dimension=1, tiled=True)  75.6 us
    unnamed x9, local copies, waits for them, and re-layouts  29.8 us
    convert_element_type x1, other arithmetic, shards(): up_low = (up_train[0] * gain_column).astype(jnp.bfloat16)  16.8 us
    squeeze x1, local copies, waits for them, and re-layouts, shards(): gate_low = (gate_train[0] * gain_column).astype(jnp.bfloat16)  14.5 us
    squeeze x1, local copies, waits for them, and re-layouts, shards(): up_low = (up_train[0] * gain_column).astype(jnp.bfloat16)  14.5 us
  transfers between devices with their start and end apart: 5, of which 4 were waited for; matrix products, arithmetic and copies ran while one was open for 13% of the time, Pallas kernels for 0%

profile of v1, /device:TPU:0, one launch (start us, length us, event | category | flops | bytes accessed | tf_op | source)
XLA Modules:
  0.0 588.0 jit_solution(3417720503515890875)
XLA Ops:
  7.2 0.8 copy.39
  8.3 1.2 reduce-window.6
  9.5 0.2 slice_reduce_fusion
  9.7 0.2 reduce-window.9
  10.0 0.1 reduce_sum.30
  10.2 0.7 multiply_add_fusion
  11.1 1.4 fusion.3
  12.4 3.3 convolution_convert_fusion
  15.7 4.2 all-to-all-start.3
  19.9 14.5 %squeeze.8 = f32[512,4,1408]{2,1,0:T(4,128)} reshape(f32[1,512,5632]{2,1,0:T(8,128)} %param.12) | data formatting | bytes 23068672 | tf_op jit(solution)/shard_map/squeeze | solution.py:16
  34.5 14.5 %squeeze.7 = f32[512,4,1408]{2,1,0:T(4,128)} reshape(f32[1,512,5632]{2,1,0:T(8,128)} %param.11) | data formatting | bytes 23068672 | tf_op jit(solution)/shard_map/squeeze | solution.py:15
  49.0 16.8 %fusion = (bf16[512,4,1408]{2,0,1:T(8,128)(2,1)}, bf16[512,4,1408]{2,0,1:T(8,128)(2,1)}) fusion(f32[512,4,1408]{2,1,0:T(4,128)} %squeeze.8, f32[512]{0:T(512)S(1)} %copy-done, f32[512,4,1408]{2,1,0:T(4,128)} %squeeze.7), kind=kLoop, calls=%fused_computation.1 | loop fusion | flops 11534336 | bytes 34605056 | tf_op jit(solution)/shard_map/convert_element_type | solution.py:16
  65.9 135.1 %all_to_all.47 = bf16[512,4,1408]{2,0,1:T(8,128)(2,1)} all-to-all(bf16[512,4,1408]{2,0,1:T(8,128)(2,1)} %get-tuple-element.21), channel_id=1, replica_groups=mesh['grp'=2,'fs'=4,'tp'=4] {'fs'}, dimensions={1} | all-to-all | bytes 11534336 | tf_op jit(solution)/shard_map/all_to_all | solution.py:22
  200.9 5.2 all-to-all-start.1
  206.1 9.6 %copy.38 = bf16[1,5632,512]{1,2,0:T(8,128)(2,1)} copy(f32[1,5632,512]{2,1,0:T(8,128)} %param.13) | data formatting | bytes 17301504 | tf_op args[6]
  215.6 3.1 fusion.14
  218.8 3.2 pad_maximum_fusion
  222.0 111.3 %all-to-all-done.1 = bf16[512,4,1408]{2,0,1:T(8,128)(2,1)} async-done(((bf16[512,4,1408]{2,0,1:T(8,128)(2,1)}), bf16[512,4,1408]{2,0,1:T(8,128)(2,1)}, u32[]{:S(2)}, u32[]{:S(2)}) %all-to-all-start.1) | async-done | bytes 5767200 | tf_op jit(solution)/shard_map/all_to_all | solution.py:23
  333.3 5.2 all-to-all-start.2
  338.5 0.2 reduce-scatter.2.cloned.1.call-start
  338.7 7.6 %fusion.15 = f32[512,1408]{1,0:T(8,128)} fusion(bf16[512,2048]{1,0:T(8,128)(2,1)S(1)} %bitcast.48, bf16[2048,1408]{1,0:T(8,128)(2,1)} %bitcast.46), kind=kOutput, calls=%fused_computation.32 | convolution fusion | flops 2952790016 | bytes 10747904 | tf_op jit(solution)/shard_map/dot_general | solution.py:52
  346.3 118.6 %all-to-all-done.2 = bf16[4,1408,512]{1,2,0:T(8,128)(2,1)} async-done(((bf16[4,1408,512]{1,2,0:T(8,128)(2,1)}), bf16[4,1408,512]{1,2,0:T(8,128)(2,1)}, u32[]{:S(2)}, u32[]{:S(2)}) %all-to-all-start.2) | async-done | bytes 5767200 | tf_op jit(solution)/shard_map/all_to_all | solution.py:26
  464.9 13.9 %fusion.8 = f32[512,2048]{1,0:T(8,128)} fusion(bf16[1408,2048]{0,1:T(8,128)(2,1)} %bitcast.11, bf16[512,2048]{1,0:T(8,128)(2,1)S(1)} %bitcast.49, bf16[2048,1408]{1,0:T(8,128)(2,1)} %bitcast.10, f32[512,1408]{1,0:T(8,128)} %fusion.15), kind=kOutput, calls=%fused_computation.18 | convolution fusion | flops 5909905408 | bytes 20709376 | tf_op jit(solution)/shard_map/dot_general | solution.py:55
  478.8 75.6 %reduce-scatter.2.cloned.1.call-done = f32[512,512]{1,0:T(8,128)} async-done(((f32[512,2048]{1,0:T(8,128)}), f32[512,512]{1,0:T(8,128)}) %reduce-scatter.2.cloned.1.call-update) | async-done | bytes 1048592 | tf_op jit(solution)/shard_map/reduce_scatter | solution.py:58
  554.4 2.1 convert_element_type.48
  556.5 3.5 all-to-all-start.4
  560.0 0.2 select_reduce_fusion
  560.2 8.2 %copy.42 = bf16[1,1408,2048]{2,1,0:T(8,128)(2,1)} copy(bf16[1,1408,2048]{1,2,0:T(8,128)(2,1)} %bitcast.5) | data formatting | bytes 11534336
  568.4 0.3 all-to-all-done.4
  568.8 1.2 convolution_convert_fusion.1
  569.9 5.6 copy.53
  575.5 5.6 copy.54
  (14 shorter events, 0.6 us)
Async XLA Ops:
  15.7 50.1 %all-to-all-start.3 = ((bf16[4,128,2048]{2,1,0:T(8,128)(2,1)}), bf16[4,128,2048]{2,1,0:T(8,128)(2,1)S(1)}, u32[]{:S(2)}, u32[]{:S(2)}) async-start(bf16[4,128,2048]{2,1,0:T(8,128)(2,1)} %bitcast.7), calls=%async_computation.3 | async-start | bytes 4194304 | tf_op jit(solution)/shard_map/all_to_all | solution.py:46
  34.5 14.5 %copy-start = (f32[512]{0:T(512)S(1)}, f32[512]{0:T(512)}, u32[]{:S(2)}) copy-start(f32[512]{0:T(512)} %param.10) | copy-start | bytes 6148
  200.9 132.4 %all-to-all-start.1 = ((bf16[512,4,1408]{2,0,1:T(8,128)(2,1)}), bf16[512,4,1408]{2,0,1:T(8,128)(2,1)}, u32[]{:S(2)}, u32[]{:S(2)}) async-start(bf16[512,4,1408]{2,0,1:T(8,128)(2,1)} %get-tuple-element.20), calls=%async_computation.1 | async-start | bytes 11534336 | tf_op jit(solution)/shard_map/all_to_all | solution.py:23
  333.3 131.6 %all-to-all-start.2 = ((bf16[4,1408,512]{1,2,0:T(8,128)(2,1)}), bf16[4,1408,512]{1,2,0:T(8,128)(2,1)}, u32[]{:S(2)}, u32[]{:S(2)}) async-start(bf16[4,1408,512]{1,2,0:T(8,128)(2,1)} %pad_maximum_fusion), calls=%async_computation.2 | async-start | bytes 11534336 | tf_op jit(solution)/shard_map/all_to_all | solution.py:26
  338.5 216.0 %reduce-scatter.2.cloned.1.call-start = ((), (), s32[]{:S(2)}) async-start(), calls=%async_computation.6 | async-start | bytes 5242880 | tf_op jit(solution)/shard_map/reduce_scatter | solution.py:58
  478.8 81.2 %copy-start.1 = (f32[192,2]{0,1:T(2,128)S(1)}, f32[192,2]{0,1:T(2,128)}, u32[]{:S(2)}) copy-start(f32[192,2]{0,1:T(2,128)} %param.9) | copy-start | bytes 4612
  556.5 12.3 %all-to-all-start.4 = ((bf16[4,128,512]{2,1,0:T(8,128)(2,1)}), bf16[4,128,512]{2,1,0:T(8,128)(2,1)S(1)}, u32[]{:S(2)}, u32[]{:S(2)}) async-start(bf16[4,128,512]{2,1,0:T(8,128)(2,1)} %bitcast.12), calls=%async_computation.5 | async-start | bytes 1048576 | tf_op jit(solution)/shard_map/all_to_all | solution.py:61
Sparse Core Ops, SparseCore 0:
  479.0 75.4 reduce-scatter.1
